TPU v7x, 512 devices: a whole 4x4x16 slice. The times are simulated.
512 devices in a mesh: kv: 32 (over z, core), tp: 16 (over y, x).
Axes of the slice: x: 4, y: 4, z: 16, core: 2. Of those that a mesh axis runs over, the one named last changes fastest.
Arguments:
- tokens: bfloat16 [16, 2048], P(None, 'kv'), may hold values from -8 to 8
- lengths: int32 [16], replicated, may hold values from 1 to 49152, 196608 in all
- latent_cache: bfloat16 [16, 49152, 256], P(None, ('kv', 'tp')), may hold values from -10 to 10
- rope_cache: bfloat16 [16, 49152, 32], P(None, ('kv', 'tp')), may hold values from -2000 to 2000
- gain_in: bfloat16 [2048], P('kv'), may hold values from 0.099609375 to 1.8984375
- w_down_q: bfloat16 [2048, 512], P('kv'), may hold values from -0.125 to 0.125
- w_down_kv: bfloat16 [2048, 256], P('kv'), may hold values from -0.125 to 0.125
- w_rope_key: bfloat16 [2048, 32], P('kv'), may hold values from -0.125 to 0.125
- gain_q: bfloat16 [512], replicated, may hold values from 0.099609375 to 1.8984375
- w_up_qn: bfloat16 [512, 16, 64], replicated, may hold values from -0.25 to 0.25
- w_up_qr: bfloat16 [512, 16, 32], replicated, may hold values from -0.25 to 0.25
- gain_kv: bfloat16 [256], replicated, may hold values from 0.099609375 to 1.8984375
- w_key_up: bfloat16 [256, 16, 64], replicated, may hold values from -0.375 to 0.375
- w_value_up: bfloat16 [256, 16, 64], replicated, may hold values from -0.375 to 0.375
- w_attn_out: bfloat16 [16, 64, 2048], P('tp', None, 'kv'), may hold values from -0.1875 to 0.1875
- gain_mid: bfloat16 [2048], P('kv'), may hold values from 0.099609375 to 1.8984375
- w_ff_in: bfloat16 [2048, 8192], P('kv', 'tp'), may hold values from -0.125 to 0.125
- w_ff_out: bfloat16 [8192, 2048], P('tp', 'kv'), may hold values from -0.0625 to 0.0625
Outputs:
- mixed: bfloat16 [16, 2048], P(None, 'kv')
- new_latent: bfloat16 [16, 256], replicated
- new_rope_key: bfloat16 [16, 32], replicated
Inputs may be any that keep to these rules, and one draw needn't show every extreme that they name: `lengths`: each sequence's live cache positions; one sequence fills the whole cache.
All inputs are finite; a program needn't handle non-finite values.
Results may differ from a plain program's by a relative error of at most 0.012.
Values sent between devices are 32-bit elements; how exact they have to be, the bound alone decides.
A program may use at most 64 MiB of HBM per device.

v0:
```python
import jax
import jax.numpy as jnp
from jax import lax
from jax.sharding import Mesh
from jax.sharding import PartitionSpec as P

D = 2048
NOPE = 64
ROPE = 32
KV = ("kv_0", "kv_1")
KV_TP = ("kv_0", "kv_1", "tp_0", "tp_1")
TP = ("tp_0", "tp_1")


EPS = 1e-06


def over_axes(value, axes):
    for axis in axes:
        value = lax.psum(value, axis)
    return value


def copy_for_each(value, axis):
    size = lax.axis_size(axis)
    return lax.all_to_all(
        jnp.broadcast_to(value[None], (size, *value.shape)), axis, 0, 0, tiled=True
    )


def gathered_once(value, axis):
    leaves = jax.tree.leaves(value)
    order = sorted(range(len(leaves)), key=lambda k: -leaves[k].size)
    width = (1, *leaves[order[0]].shape)[-1]
    lines = [
        jnp.pad(leaves[k].reshape(-1), (0, -leaves[k].size % width)).reshape(-1, width)
        for k in order
    ]
    both, at, found = (copy_for_each(jnp.concatenate(lines), axis), 0, {})
    for k, line in zip(order, lines):
        piece = both[:, at : at + len(line)].reshape(len(both), -1)
        found[k] = piece[:, : leaves[k].size].reshape(-1, *leaves[k].shape)
        at += len(line)
    numbers = iter(range(len(leaves)))
    return jax.tree.map(lambda _: found[next(numbers)], value)


def joined_by_halves(pieces, combine):
    while len(jax.tree.leaves(pieces)[0]) > 1:
        pieces = jax.vmap(combine)(
            *(jax.tree.map(lambda part: part[side::2], pieces) for side in (0, 1))
        )
    return jax.tree.map(lambda part: part[0], pieces)


def joined_all(value, axis, combine):
    pieces = gathered_once(value, axis)
    return joined_by_halves(pieces, combine)


def of_everyone(value, axis):
    everything = copy_for_each(value, axis)
    return jnp.sum(everything, axis=0)


def in_one(arrays, axis):
    ravelled, at, outs = (jnp.concatenate([a.reshape(-1) for a in arrays]), 0, [])
    subtotal = of_everyone(ravelled, axis)
    for a in arrays:
        outs.append(subtotal[at : at + a.size].reshape(a.shape))
        at += a.size
    return tuple(outs)


def rotate(values, positions):
    half = values.shape[-1] // 2
    inverse = 10000.0 ** (-jnp.arange(half, dtype=jnp.float32) / half)
    angle = positions.astype(jnp.float32)[:, None, None] * inverse[None, None, :]
    first = values[..., :half]
    second = values[..., half:]
    return jnp.concatenate(
        [
            first * jnp.cos(angle) - second * jnp.sin(angle),
            second * jnp.cos(angle) + first * jnp.sin(angle),
        ],
        axis=-1,
    )


def rms_scaled(values, gain):
    return (
        values
        * lax.rsqrt(jnp.mean(values * values, axis=-1, keepdims=True) + EPS)
        * gain.astype(jnp.float32)
    )


def combine(earlier, later):
    top_a, total_a, acc_a = earlier
    top_b, total_b, acc_b = later
    top = jnp.maximum(top_a, top_b)
    fade_a = jnp.exp(top_a - top)
    fade_b = jnp.exp(top_b - top)
    return (
        top,
        total_a * fade_a + total_b * fade_b,
        acc_a * fade_a[..., None] + acc_b * fade_b[..., None],
    )


def fold_sources(parts):
    tops, totals, accs = parts
    top = jnp.max(tops, axis=0)
    fade = jnp.exp(tops - top[None])
    return (top, jnp.sum(totals * fade, axis=0), jnp.sum(accs * fade[..., None], axis=0))


def per_device(
    tokens,
    lengths,
    latent_cache,
    rope_cache,
    gain_in,
    w_down_q,
    w_down_kv,
    w_rope_key,
    gain_q,
    w_up_qn,
    w_up_qr,
    gain_kv,
    w_key_up,
    w_value_up,
    w_attn_out,
    gain_mid,
    w_ff_in,
    w_ff_out,
):
    f32 = jnp.float32
    bf16 = jnp.bfloat16
    scale = (NOPE + ROPE) ** (-0.5)
    resid = tokens.astype(f32)
    scaled_in = (resid * gain_in.astype(f32)).astype(bf16)
    part_q = jnp.dot(scaled_in, w_down_q, preferred_element_type=f32)
    part_kv = jnp.dot(scaled_in, w_down_kv, preferred_element_type=f32)
    part_rope = jnp.dot(scaled_in, w_rope_key, preferred_element_type=f32)
    square_in = jnp.sum(resid * resid, axis=1)
    sum_q, sum_kv, sum_rope, total_in = (
        over_axes(part_q, KV),
        over_axes(part_kv, KV),
        over_axes(part_rope, KV),
        over_axes(square_in, KV),
    )
    inv_in = lax.rsqrt(total_in / D + EPS)[:, None]
    query_latent = rms_scaled(inv_in * sum_q, gain_q).astype(bf16)
    new_latent = rms_scaled(inv_in * sum_kv, gain_kv).astype(bf16)
    new_rope_key = rotate((inv_in * sum_rope)[:, None, :], lengths)[:, 0, :].astype(bf16)
    query_nope = jnp.einsum(
        "bc,chd->bhd", query_latent, w_up_qn, preferred_element_type=f32
    ).astype(bf16)
    query_rope = rotate(
        jnp.einsum("bc,chr->bhr", query_latent, w_up_qr, preferred_element_type=f32), lengths
    ).astype(bf16)
    query_cache = jnp.einsum(
        "bhd,khd->bhk", query_nope, w_key_up, preferred_element_type=f32
    ).astype(bf16)
    rows = latent_cache.shape[1]
    positions = lax.axis_index(KV_TP) * rows + jnp.arange(rows, dtype=jnp.int32)
    live = (positions[None, :] < lengths[:, None])[:, None, :]
    scores = (
        jnp.einsum("bhk,blk->bhl", query_cache, latent_cache, preferred_element_type=f32)
        + jnp.einsum("bhr,blr->bhl", query_rope, rope_cache, preferred_element_type=f32)
    ) * scale
    scores = jnp.where(live, scores, -1e30)
    top = jnp.max(scores, axis=2)
    weights = jnp.where(live, jnp.exp(scores - top[:, :, None]), 0.0)
    total = jnp.sum(weights, axis=2)
    acc = jnp.einsum("bhl,blk->bhk", weights.astype(bf16), latent_cache, preferred_element_type=f32)
    heads_dev = w_attn_out.shape[0]
    first_head = lax.axis_index(TP) * heads_dev
    own_value_up = lax.dynamic_slice_in_dim(w_value_up, first_head, heads_dev, 1).astype(f32)
    own_cache_q = lax.dynamic_slice_in_dim(query_cache, first_head, heads_dev, 1)
    own_rope_q = lax.dynamic_slice_in_dim(query_rope, first_head, heads_dev, 1)
    self_score = (
        jnp.einsum("bhk,bk->bh", own_cache_q, new_latent, preferred_element_type=f32)
        + jnp.einsum("bhr,br->bh", own_rope_q, new_rope_key, preferred_element_type=f32)
    ) * scale
    expanded = jnp.einsum("bhk,khv->bhv", acc, w_value_up.astype(f32))
    top, total, expanded = fold_sources(
        (
            lax.all_to_all(top[None], TP, split_axis=2, concat_axis=0, tiled=True),
            lax.all_to_all(total[None], TP, split_axis=2, concat_axis=0, tiled=True),
            lax.all_to_all(expanded[None], TP, split_axis=2, concat_axis=0, tiled=True),
        )
    )
    top, total, expanded = joined_all((top, total, expanded), KV, combine)
    joined = jnp.maximum(top, self_score)
    fade = jnp.exp(top - joined)
    self_weight = jnp.exp(self_score - joined)
    total = total * fade + self_weight
    self_value = jnp.einsum("bk,khv->bhv", new_latent.astype(f32), own_value_up)
    expanded = (
        expanded * fade[:, :, None] + self_weight.astype(bf16).astype(f32)[:, :, None] * self_value
    )
    head_out = (expanded / total[:, :, None]).astype(bf16)
    attn_part = jnp.einsum("bhv,hvd->bd", head_out, w_attn_out, preferred_element_type=f32)
    resid_mid = resid + over_axes(attn_part, TP)
    scaled_mid = (resid_mid * gain_mid.astype(f32)).astype(bf16)
    hidden_part = jnp.dot(scaled_mid, w_ff_in, preferred_element_type=f32)
    square_mid = jnp.sum(resid_mid * resid_mid, axis=1)
    hidden_sum, total_mid = in_one((hidden_part, square_mid), KV)
    inv_mid = lax.rsqrt(total_mid / D + EPS)[:, None]
    hidden = jnp.square(jax.nn.relu(inv_mid * hidden_sum)).astype(bf16)
    out_part = jnp.dot(hidden, w_ff_out, preferred_element_type=f32)
    mixed = (resid_mid + over_axes(out_part, TP)).astype(bf16)
    return (mixed, new_latent, new_rope_key)


def solution(mesh):
    finer = Mesh(mesh.devices.reshape(16, 2, 4, 4), ("kv_0", "kv_1", "tp_0", "tp_1"))
    in_specs = (
        P(None, KV),
        P(),
        P(None, KV_TP, None),
        P(None, KV_TP, None),
        P(KV),
        P(KV, None),
        P(KV, None),
        P(KV, None),
        P(),
        P(),
        P(),
        P(),
        P(),
        P(),
        P(TP, None, KV),
        P(KV),
        P(KV, TP),
        P(TP, KV),
    )
    out_specs = (P(None, KV), P(), P())
    return jax.shard_map(
        per_device, mesh=finer, in_specs=in_specs, out_specs=out_specs, check_vma=False
    )
```

profile of v0, /device:TPU:1, one launch (start us, length us, event | category | flops | bytes accessed | tf_op | source)
XLA Modules:
  0.0 237.1 jit_solution(12234813138934605315)
XLA Ops:
  0.7 0.8 convert_element_type.73
  1.5 0.7 convert_element_type.80
  2.1 0.8 fusion.36
  2.9 0.7 broadcast_compare_fusion
  3.7 0.7 convert_element_type.75
  4.3 0.8 fusion.55
  5.2 0.9 fusion.57
  6.1 1.0 fusion.59
  7.1 49.2 %all-reduce.2 = (f32[16,256]{1,0:T(8,128)S(1)}, f32[16]{0:T(128)S(1)}, f32[16,512]{1,0:T(8,128)S(1)}, f32[16,32]{1,0:T(8,128)S(1)}) all-reduce(f32[16,256]{1,0:T(8,128)S(1)} %fusion.57, f32[16]{0:T(128)S(1)} %fusion.36, f32[16,512]{1,0:T(8,128)S(1)} %fusion.59, ...), channel_id=1, replica_groups=mesh['kv_0'=16,'kv_1'=2,'tp_0'=4,'tp_1'=4] {'kv_0'}, use_global_device_ids=true, to_apply=%region_11.12 | all-reduce | flops 12816 | bytes 102528 | tf_op jit(solution)/shard_map/psum | solution.py:20
  56.2 17.8 %all-reduce.3 = (f32[16,256]{1,0:T(8,128)S(1)}, f32[16]{0:T(128)S(1)}, f32[16,512]{1,0:T(8,128)S(1)}, f32[16,32]{1,0:T(8,128)S(1)}) all-reduce(f32[16,256]{1,0:T(8,128)S(1)} %get-tuple-element.3, f32[16]{0:T(128)S(1)} %get-tuple-element.4, ...), channel_id=1, replica_groups=mesh['kv_0'=16,'kv_1'=2,'tp_0'=4,'tp_1'=4] {'kv_1'}, use_global_device_ids=true, to_apply=%region_12.13 | all-reduce | flops 12816 | bytes 102528 | tf_op jit(solution)/shard_map/psum | solution.py:20
  74.4 1.5 fusion.78
  76.0 0.7 convolution_convert_fusion
  77.5 0.7 copy.58
  78.2 6.8 %all-to-all-start.1 = ((f32[1,16,16]{1,0,2:T(1,128)}), f32[1,16,16]{1,0,2:T(1,128)S(1)}, u32[]{:S(2)}, u32[]{:S(2)}) async-start(f32[1,16,16]{1,0,2:T(1,128)} %copy.58), calls=%async_computation.1 | async-start | bytes 16384 | tf_op jit(solution)/shard_map/all_to_all | solution.py:190
  85.9 0.7 reshape.385
  86.7 0.7 copy.59
  87.4 4.0 %all-to-all-done.1 = f32[1,16,16]{1,0,2:T(1,128)S(1)} async-done(((f32[1,16,16]{1,0,2:T(1,128)}), f32[1,16,16]{1,0,2:T(1,128)S(1)}, u32[]{:S(2)}, u32[]{:S(2)}) %all-to-all-start.1) | async-done | bytes 1056 | tf_op jit(solution)/shard_map/all_to_all | solution.py:190
  91.4 3.4 %all-to-all-start.2 = ((f32[1,16,16]{1,0,2:T(1,128)}), f32[1,16,16]{1,0,2:T(1,128)S(1)}, u32[]{:S(2)}, u32[]{:S(2)}) async-start(f32[1,16,16]{1,0,2:T(1,128)} %copy.59), calls=%async_computation.2 | async-start | bytes 16384 | tf_op jit(solution)/shard_map/all_to_all | solution.py:191
  94.9 6.3 %all-to-all-done.2 = f32[1,16,16]{1,0,2:T(1,128)S(1)} async-done(((f32[1,16,16]{1,0,2:T(1,128)}), f32[1,16,16]{1,0,2:T(1,128)S(1)}, u32[]{:S(2)}, u32[]{:S(2)}) %all-to-all-start.2) | async-done | bytes 1056 | tf_op jit(solution)/shard_map/all_to_all | solution.py:191
  101.2 3.5 %all-to-all-start = ((f32[16,1,1024]{2,1,0:T(1,128)}), f32[16,1,1024]{2,1,0:T(1,128)S(1)}, u32[]{:S(2)}, u32[]{:S(2)}) async-start(f32[16,1,1024]{2,1,0:T(1,128)} %reshape.385), calls=%async_computation | async-start | bytes 131072 | tf_op jit(solution)/shard_map/all_to_all | solution.py:192
  104.7 6.4 %all-to-all-done = f32[16,1,1024]{2,1,0:T(1,128)S(1)} async-done(((f32[16,1,1024]{2,1,0:T(1,128)}), f32[16,1,1024]{2,1,0:T(1,128)S(1)}, u32[]{:S(2)}, u32[]{:S(2)}) %all-to-all-start) | async-done | bytes 65568 | tf_op jit(solution)/shard_map/all_to_all | solution.py:192
  111.7 0.8 reduce.11
  112.7 0.8 reshape.387
  113.5 10.5 %all-to-all-start.3 = ((f32[32,1,1152]{2,1,0:T(1,128)}), f32[32,1,1152]{2,1,0:T(1,128)S(1)}, u32[]{:S(2)}, u32[]{:S(2)}) async-start(f32[32,1,1152]{2,1,0:T(1,128)} %reshape.387), calls=%async_computation.3 | async-start | bytes 294912 | tf_op jit(solution)/shard_map/all_to_all | solution.py:26
  124.0 0.8 fusion.45
  125.3 15.2 %all-to-all-done.3 = f32[32,1,1152]{2,1,0:T(1,128)S(1)} async-done(((f32[32,1,1152]{2,1,0:T(1,128)}), f32[32,1,1152]{2,1,0:T(1,128)S(1)}, u32[]{:S(2)}, u32[]{:S(2)}) %all-to-all-start.3) | async-done | bytes 147488 | tf_op jit(solution)/shard_map/all_to_all | solution.py:26
  140.5 1.0 reduce.12
  142.9 6.9 %psum.92 = f32[16,64]{1,0:T(8,128)S(1)} all-reduce(f32[16,64]{1,0:T(8,128)S(1)} %fusion.5), channel_id=1, replica_groups=mesh['kv_0'=16,'kv_1'=2,'tp_0'=4,'tp_1'=4] {'tp_0'}, use_global_device_ids=true, to_apply=%region_16.17 | all-reduce | flops 1024 | bytes 8192 | tf_op jit(solution)/shard_map/psum | solution.py:20
  149.8 7.0 %psum.93 = f32[16,64]{1,0:T(8,128)S(1)} all-reduce(f32[16,64]{1,0:T(8,128)S(1)} %psum.92), channel_id=1, replica_groups=mesh['kv_0'=16,'kv_1'=2,'tp_0'=4,'tp_1'=4] {'tp_1'}, use_global_device_ids=true, to_apply=%region_17.18 | all-reduce | flops 1024 | bytes 8192 | tf_op jit(solution)/shard_map/psum | solution.py:20
  157.6 64.4 %all_to_all.68 = f32[32,1,8208]{2,1,0:T(1,128)S(1)} all-to-all(f32[32,1,8208]{2,1,0:T(1,128)S(1)} %broadcast_in_dim.38), channel_id=1, replica_groups=mesh['kv_0'=16,'kv_1'=2,'tp_0'=4,'tp_1'=4] {'kv_0','kv_1'}, dimensions={0} | all-to-all | bytes 2101248 | tf_op jit(solution)/shard_map/all_to_all | solution.py:26
  223.1 6.7 %psum.94 = f32[16,64]{1,0:T(8,128)S(1)} all-reduce(f32[16,64]{1,0:T(8,128)S(1)} %fusion.23), channel_id=1, replica_groups=mesh['kv_0'=16,'kv_1'=2,'tp_0'=4,'tp_1'=4] {'tp_0'}, use_global_device_ids=true, to_apply=%region_20.21 | all-reduce | flops 1024 | bytes 8192 | tf_op jit(solution)/shard_map/psum | solution.py:20
  229.8 6.7 %psum.95 = f32[16,64]{1,0:T(8,128)S(1)} all-reduce(f32[16,64]{1,0:T(8,128)S(1)} %psum.94), channel_id=1, replica_groups=mesh['kv_0'=16,'kv_1'=2,'tp_0'=4,'tp_1'=4] {'tp_1'}, use_global_device_ids=true, to_apply=%region_21.22 | all-reduce | flops 1024 | bytes 8192 | tf_op jit(solution)/shard_map/psum | solution.py:20
  (103 shorter events, 7.0 us)
Async XLA Ops:
  0.6 75.3 %copy-start = (bf16[512,16,64]{0,2,1:T(8,128)(2,1)S(1)}, bf16[512,16,64]{0,2,1:T(8,128)(2,1)}, u32[]{:S(2)}) copy-start(bf16[512,16,64]{0,2,1:T(8,128)(2,1)} %param.27) | copy-start | bytes 3145732
  0.6 75.3 %copy-start.3 = (bf16[256,16,64]{0,2,1:T(8,128)(2,1)S(1)}, bf16[256,16,64]{0,2,1:T(8,128)(2,1)}, u32[]{:S(2)}) copy-start(bf16[256,16,64]{0,2,1:T(8,128)(2,1)} %param.30) | copy-start | bytes 1572868
  75.9 0.9 copy-start.5
  76.0 1.2 copy-start.1
  77.2 8.3 %copy-start.2 = (bf16[256,16,64]{0,2,1:T(8,128)(2,1)S(1)}, bf16[256,16,64]{0,2,1:T(8,128)(2,1)}, u32[]{:S(2)}) copy-start(bf16[256,16,64]{0,2,1:T(8,128)(2,1)} %param.31) | copy-start | bytes 1572868
  78.2 13.1 %all-to-all-start.1 = ((f32[1,16,16]{1,0,2:T(1,128)}), f32[1,16,16]{1,0,2:T(1,128)S(1)}, u32[]{:S(2)}, u32[]{:S(2)}) async-start(f32[1,16,16]{1,0,2:T(1,128)} %copy.58), calls=%async_computation.1 | async-start | bytes 16384 | tf_op jit(solution)/shard_map/all_to_all | solution.py:190
  86.7 38.1 %copy-start.10 = (bf16[64]{0:T(256)(128)(2,1)S(1)}, bf16[64]{0:T(256)(128)(2,1)}, u32[]{:S(2)}) copy-start(bf16[64]{0:T(256)(128)(2,1)} %param.33) | copy-start | bytes 388
  86.7 38.1 %copy-start.11 = (bf16[256]{0:T(256)(128)(2,1)S(1)}, bf16[256]{0:T(256)(128)(2,1)}, u32[]{:S(2)}) copy-start(bf16[256]{0:T(256)(128)(2,1)} %param.29) | copy-start | bytes 1540
  91.4 9.8 %all-to-all-start.2 = ((f32[1,16,16]{1,0,2:T(1,128)}), f32[1,16,16]{1,0,2:T(1,128)S(1)}, u32[]{:S(2)}, u32[]{:S(2)}) async-start(f32[1,16,16]{1,0,2:T(1,128)} %copy.59), calls=%async_computation.2 | async-start | bytes 16384 | tf_op jit(solution)/shard_map/all_to_all | solution.py:191
  101.2 10.0 %all-to-all-start = ((f32[16,1,1024]{2,1,0:T(1,128)}), f32[16,1,1024]{2,1,0:T(1,128)S(1)}, u32[]{:S(2)}, u32[]{:S(2)}) async-start(f32[16,1,1024]{2,1,0:T(1,128)} %reshape.385), calls=%async_computation | async-start | bytes 131072 | tf_op jit(solution)/shard_map/all_to_all | solution.py:192
  113.5 26.9 %all-to-all-start.3 = ((f32[32,1,1152]{2,1,0:T(1,128)}), f32[32,1,1152]{2,1,0:T(1,128)S(1)}, u32[]{:S(2)}, u32[]{:S(2)}) async-start(f32[32,1,1152]{2,1,0:T(1,128)} %reshape.387), calls=%async_computation.3 | async-start | bytes 294912 | tf_op jit(solution)/shard_map/all_to_all | solution.py:26
  125.2 17.4 %copy-start.7 = (bf16[16,256]{1,0:T(8,128)(2,1)}, bf16[16,256]{1,0:T(8,128)(2,1)S(1)}, u32[]{:S(2)}) copy-start(bf16[16,256]{1,0:T(8,128)(2,1)S(1)} %get-tuple-element.28) | copy-start | bytes 24580
  141.5 1.1 copy-start.9
  141.6 15.2 %copy-start.4 = (bf16[16,64]{1,0:T(8,128)(2,1)S(1)}, bf16[16,64]{1,0:T(8,128)(2,1)}, u32[]{:S(2)}) copy-start(bf16[16,64]{1,0:T(8,128)(2,1)} %param.18) | copy-start | bytes 6148
  141.6 15.3 %copy-start.6 = (bf16[64,512]{1,0:T(8,128)(2,1)S(1)}, bf16[64,512]{1,0:T(8,128)(2,1)}, u32[]{:S(2)}) copy-start(bf16[64,512]{1,0:T(8,128)(2,1)} %param.34) | copy-start | bytes 196612
  222.1 0.8 copy-start.8
where the time goes:
time: 242 us; the launch traced here: 237 us
  blocking collectives  159 us (66%)
  waiting for transfers between devices  31.9 us (13%)
  starting transfers between devices  24.2 us (10%)
  other arithmetic  9.57 us (4%)
  matrix products  6.51 us (3%)
  local copies, waits for them, and re-layouts  5 us (2%)
    psum x6, blocking collectives, over_axes(): value = lax.psum(value, axis)  94.3 us
    all_to_all x1, blocking collectives, copy_for_each(): lax.all_to_all(jnp.broadcast_to(value[None], (size, *value.shape)), axis,...  64.4 us
    all_to_all x1, waiting for transfers between devices, copy_for_each(): lax.all_to_all(jnp.broadcast_to(value[None], (size, *value.shape)), axis,...  15.2 us
    all_to_all x1, starting transfers between devices, copy_for_each(): lax.all_to_all(jnp.broadcast_to(value[None], (size, *value.shape)), axis,...  10.5 us
    all_to_all x1, starting transfers between devices, per_device(): lax.all_to_all(top[None], TP, split_axis=2, concat_axis=0, tiled=True)  6.75 us
    all_to_all x1, waiting for transfers between devices, per_device(): lax.all_to_all(expanded[None], TP, split_axis=2, concat_axis=0, tiled=True)  6.42 us
    all_to_all x1, waiting for transfers between devices, per_device(): lax.all_to_all(total[None], TP, split_axis=2, concat_axis=0, tiled=True)  6.32 us
  transfers between devices with their start and end apart: 4, of which 4 were waited for; matrix products, arithmetic and copies ran while one was open for 2% of the time, Pallas kernels for 0%

commit v1 on v0

v1 whole, which is shorter than its diff:
```python
import functools

import jax
import jax.numpy as jnp
import numpy as np
from jax import lax
from jax.experimental import pallas as pl
from jax.experimental.pallas import tpu as pltpu
from jax.sharding import Mesh
from jax.sharding import PartitionSpec as P

D = 2048
H = 16
NOPE = 64
ROPE = 32
NZ = 16
NT = 16
SEQS = 16
SPAN = 96
KR = 256
EPS = 1e-06
SCALE = (NOPE + ROPE) ** (-0.5)
MESH = pl.DeviceIdType.MESH
f32 = jnp.float32
bf16 = jnp.bfloat16

Z_OFFSETS = sorted(range(1, NZ), key=lambda d: -min(d, NZ - d))


def torus_distance(d):
    y, x = d // 4, d % 4
    return min(y, 4 - y) + min(x, 4 - x)


def nt(a, b):
    return lax.dot_general(a, b, (((1,), (1,)), ((), ())), preferred_element_type=f32)


def nn(a, b):
    return jnp.dot(a, b, preferred_element_type=f32)


def rotated(x, cos, sin, low):
    n = x.shape[-1]
    swapped = jnp.where(low, pltpu.roll(x, n - 16, 1), pltpu.roll(x, 16, 1))
    return x * cos + swapped * sin


def merged(pieces, lane):
    tops = [jnp.broadcast_to(p[:, 64:65], p.shape) for p in pieces]
    top = functools.reduce(jnp.maximum, tops)
    out = None
    for p, own in zip(pieces, tops):
        term = p * jnp.exp(own - top)
        out = term if out is None else out + term
    return top, jnp.where(lane == 64, top, out)


def kernel(
    tokens,
    lengths,
    latent,
    rope,
    gain_in,
    w_q,
    w_kv,
    w_rope,
    gain_q,
    w_qn,
    w_qr,
    gain_kv,
    w_k,
    w_v,
    w_ao,
    gain_mid,
    w_in,
    w_out,
    freq,
    mixed,
    new_latent,
    new_rope,
    tokens_s,
    lengths_s,
    latent_s,
    rope_s,
    gain_in_s,
    w_q_s,
    w_kv_s,
    w_rope_s,
    gain_q_s,
    w_qn_s,
    w_qr_s,
    gain_kv_s,
    w_k_s,
    w_v_s,
    w_ao_s,
    gain_mid_s,
    w_in_s,
    w_out_s,
    freq_s,
    part_s,
    pair_a,
    pair_small,
    pair_big,
    a1,
    a2,
    qc_s,
    qr_s,
    acc_s,
    st_s,
    nl_s,
    b_send,
    b_recv,
    c_recv,
    d_recv,
    rm_all,
    e_send,
    e_recv,
    g_recv,
    hid_s,
    f_recv,
    load_sem,
    send_sem,
    recv_sem,
):
    z, c, t = lax.axis_index("z"), lax.axis_index("core"), lax.axis_index("tp")
    other = 1 - c
    barrier = pltpu.get_barrier_semaphore()
    z_peers = [(lax.rem(z + d, NZ), c, t) for d in Z_OFFSETS]
    t_order = sorted(range(1, NT), key=lambda d: -torus_distance(d))
    t_peers = [lax.rem(t // 4 + d // 4, 4) * 4 + lax.rem(lax.rem(t, 4) + d % 4, 4) for d in t_order]
    plane_peers = [(z, k, u) for u in t_peers for k in (c, other)] + [(z, other, t)]
    partner = (z, other, t)
    slot = 2 * t + c

    for peer in z_peers + plane_peers:
        pl.semaphore_signal(barrier, inc=1, device_id=peer, device_id_type=MESH)

    sources = (tokens, gain_in, w_q, w_kv, w_rope, lengths, freq, w_in, w_out, w_ao, gain_mid, gain_q, gain_kv, w_qn, w_qr, w_k, latent, rope, w_v)
    targets = (tokens_s, gain_in_s, w_q_s, w_kv_s, w_rope_s, lengths_s, freq_s, w_in_s, w_out_s, w_ao_s, gain_mid_s, gain_q_s, gain_kv_s, w_qn_s, w_qr_s, w_k_s, latent_s, rope_s, w_v_s)
    loads = [
        pltpu.make_async_copy(source, target, load_sem.at[i])
        for i, (source, target) in enumerate(zip(sources, targets))
    ]
    for load in loads:
        load.start()

    def send(source, target, phase, device):
        pltpu.make_async_remote_copy(
            source, target, send_sem.at[phase], recv_sem.at[phase], device_id=device, device_id_type=MESH
        ).start()

    def arrived(ref, phase):
        pltpu.make_async_copy(ref, ref, recv_sem.at[phase]).wait()

    def sent(ref, phase):
        pltpu.make_async_copy(ref, ref, send_sem.at[phase]).wait()

    lane = lax.broadcasted_iota(jnp.int32, (8, 128), 1)
    lane16 = lax.broadcasted_iota(jnp.int32, (16, 128), 1)

    for load in loads[:5]:
        load.wait()
    resid = tokens_s[...].astype(f32)
    scaled_in = (resid * gain_in_s[...].reshape(1, 64).astype(f32)).astype(bf16)
    square_in = jnp.sum(resid * resid, axis=1, keepdims=True)
    part_q = nn(scaled_in, w_q_s[...])
    part_kv = nn(scaled_in, w_kv_s[...])
    part_rope = nt(scaled_in, w_rope_s[...])
    part_rope = jnp.concatenate([part_rope, jnp.zeros((16, 96), f32)], axis=1)
    part_rope = jnp.where(lane16 == 32, square_in, part_rope)
    groups = [part_q[:, 128 * i : 128 * i + 128] for i in range(4)]
    groups += [part_kv[:, :128], part_kv[:, 128:], part_rope, jnp.zeros((16, 128), f32)]
    for g in range(8):
        for q in range(4):
            part_s[4 * g + q] = groups[g][4 * q : 4 * q + 4]

    for load in loads[5:11]:
        load.wait()
    own_lanes = lane16 // 64 == c
    twice = jnp.concatenate([resid, resid], axis=1)
    pair_small[c, 0:16] = jnp.where(own_lanes, twice, 0.0)
    ao = w_ao_s[0].astype(f32)
    ao = jnp.concatenate([ao, ao], axis=1)
    for i in range(4):
        pair_small[c, 16 + 16 * i : 32 + 16 * i] = jnp.where(own_lanes, ao[16 * i : 16 * i + 16], 0.0)
    gm = gain_mid_s[...].reshape(1, 64).astype(f32)
    gm = jnp.concatenate([gm, gm], axis=1)
    pair_small[c, 80:88] = jnp.where(lane // 64 == c, gm, 0.0)
    pair_big[c, 0:64] = w_in_s[...].astype(f32)
    pair_big[c, 64:128] = w_out_s[...].astype(f32)

    row16 = lax.broadcasted_iota(jnp.int32, (16, 128), 0)
    position = jnp.zeros((16, 128), f32)
    for b in range(SEQS):
        position = jnp.where(row16 == b, lengths_s[b].astype(f32), position)
    angle = position * freq_s[0:1, :]
    low = lax.rem(lane16, 32) < 16
    cos = jnp.cos(angle)
    sin = jnp.sin(angle)
    sin = jnp.where(low, -sin, sin)

    pl.semaphore_wait(barrier, len(z_peers) + len(plane_peers))

    send(part_s.at[2 * t + other], pair_a, 0, partner)
    arrived(pair_a, 0)
    a1[z] = part_s[slot] + pair_a[...]
    for peer in z_peers:
        send(a1.at[z], a1.at[z], 1, peer)
    send(pair_small.at[c], pair_small.at[c], 2, partner)
    send(pair_big.at[c], pair_big.at[c], 3, partner)
    for load in loads[11:]:
        load.wait()
    arrived(a1.at[pl.ds(0, NZ - 1)], 1)
    total = a1[0]
    for i in range(1, NZ):
        total = total + a1[i]
    a2[slot] = total
    for peer in plane_peers:
        send(a2.at[slot], a2.at[slot], 4, peer)
    arrived(a2.at[pl.ds(0, 31)], 4)

    def group(g):
        return jnp.concatenate([a2[4 * g + q] for q in range(4)], axis=0)

    last = group(6)
    raw_q = jnp.concatenate([group(g) for g in range(4)], axis=1)
    raw_kv = jnp.concatenate([group(4), group(5)], axis=1)
    total_in = last[:, 32:33]
    inv_in = lax.rsqrt(total_in / D + EPS)
    mean_q = jnp.sum(raw_q * raw_q, axis=1, keepdims=True) * (1.0 / 512)
    mean_kv = jnp.sum(raw_kv * raw_kv, axis=1, keepdims=True) * (1.0 / 256)
    scale_q = inv_in * lax.rsqrt(inv_in * inv_in * mean_q + EPS)
    scale_kv = inv_in * lax.rsqrt(inv_in * inv_in * mean_kv + EPS)
    query_latent = (raw_q * scale_q * gain_q_s[...].reshape(1, 512).astype(f32)).astype(bf16)
    latent_new = (raw_kv * scale_kv * gain_kv_s[...].reshape(1, 256).astype(f32)).astype(bf16)
    rope_new = rotated(last * inv_in, cos, sin, low).astype(bf16)
    new_latent[...] = latent_new
    new_rope[...] = rope_new[:, :32]
    nl_s[:, 0:256] = latent_new.astype(f32)
    nl_s[:, 256:384] = jnp.where(lane16 < 32, rope_new.astype(f32), 0.0)

    query_nope = nt(query_latent, w_qn_s[...])
    query_rope = nt(query_latent, w_qr_s[...])
    for p in range(8):
        pair = query_nope[:, 128 * p : 128 * p + 128]
        both = jnp.concatenate([jnp.where(lane16 < 64, pair, 0.0), jnp.where(lane16 < 64, 0.0, pair)], axis=0)
        both = nn(both.astype(bf16), w_k_s[128 * p : 128 * p + 128, :])
        both = both.astype(bf16).astype(f32)
        for k in (0, 1):
            qc_s[k, 32 * p : 32 * p + 32, :] = both[:, 128 * k : 128 * k + 128]
    for j in range(4):
        tile = rotated(query_rope[:, 128 * j : 128 * j + 128], cos, sin, low).astype(bf16).astype(f32)
        for i in range(4):
            h = 4 * j + i
            qr_s[16 * h : 16 * h + 16, :] = jnp.where(lane16 // 32 == i, tile, 0.0)

    first = ((2 * z + c) * NT + t) * SPAN
    spot = first + lax.broadcasted_iota(jnp.int32, (16, SPAN), 1)
    scores = []
    for b in range(SEQS):
        qc = jnp.concatenate([qc_s[k, pl.ds(b, 16, stride=16), :] for k in (0, 1)], axis=1).astype(bf16)
        qr = qr_s[pl.ds(b, 16, stride=16), :].astype(bf16)
        keys = rope_s[b]
        keys = jnp.concatenate([keys, keys, keys, keys], axis=0)
        s = (nt(qc, latent_s[b]) + nn(qr, keys)) * SCALE
        scores.append(jnp.where(spot < lengths_s[b], s, -1e30))
    for b in range(SEQS):
        s = scores[b]
        top = jnp.max(s, axis=1, keepdims=True)
        w = jnp.where(spot < lengths_s[b], jnp.exp(s - top), 0.0)
        tot = jnp.sum(w, axis=1, keepdims=True)
        acc = nn(w.astype(bf16), latent_s[b])
        for k in (0, 1):
            acc_s[k, 16 * b : 16 * b + 16, :] = acc[:, 128 * k : 128 * k + 128]
        st_s[16 * b : 16 * b + 16, :] = jnp.where(lane16 == 64, top, jnp.where(lane16 == 65, tot, 0.0))
    for p in range(8):
        wv = w_v_s[128 * p : 128 * p + 128, :]
        rows = [
            jnp.concatenate([acc_s[i, pl.ds(2 * p + k, 16, stride=16), :] for i in (0, 1)], axis=1)
            for k in (0, 1)
        ]
        both = nt(jnp.concatenate(rows, axis=0).astype(bf16), wv)
        for k in (0, 1):
            h = 2 * p + k
            value = both[16 * k : 16 * k + 16]
            if k:
                value = pltpu.roll(value, 64, 1)
            message = jnp.where(lane16 < 64, value, st_s[pl.ds(h, 16, stride=16), :])
            b_send[2 * h] = message[0:8]
            b_send[2 * h + 1] = message[8:16]
    for peer in plane_peers:
        send(b_send.at[2 * peer[2] + peer[1]], b_recv.at[slot], 5, peer)
    b_recv[slot] = b_send[slot]

    rows = pl.ds(pl.multiple_of(8 * c, 8), 8)
    head_rows = pl.ds(pl.multiple_of(16 * t + 8 * c, 8), 8)
    own_latent = nl_s[rows, 0:256]
    own_rope = nl_s[rows, 256:384]
    q_rope = qr_s[head_rows, :]
    q_rope = q_rope + pltpu.roll(q_rope, 64, 1)
    q_rope = q_rope + pltpu.roll(q_rope, 32, 1)
    own_query = jnp.concatenate([qc_s[k, head_rows, :] for k in (0, 1)], axis=1)
    self_score = SCALE * (
        jnp.sum(own_query * own_latent, axis=1, keepdims=True)
        + jnp.sum(q_rope * own_rope, axis=1, keepdims=True)
    )
    own_wv = w_v_s[pl.ds(pl.multiple_of(64 * t, 64), 64), :]
    self_value = nt(own_latent.astype(bf16), own_wv)
    self_value = jnp.concatenate([self_value, jnp.zeros((8, 64), f32)], axis=1)

    arrived(b_recv.at[pl.ds(0, 31)], 5)
    _, message = merged([b_recv[i] for i in range(32)], lane)
    c_recv[z] = message
    for peer in z_peers:
        send(c_recv.at[z], c_recv.at[z], 6, peer)

    arrived(pair_small.at[c], 2)
    arrived(pair_big.at[c], 3)
    w_ao2 = (pair_small[0, 16:80] + pair_small[1, 16:80]).astype(bf16)
    gain2 = pair_small[0, 80:88] + pair_small[1, 80:88]
    resid2 = pair_small[0, rows, :] + pair_small[1, rows, :]
    w_in2 = jnp.concatenate([pair_big[0, 0:64], pair_big[1, 0:64]], axis=0).astype(bf16)
    w_out2 = jnp.concatenate([pair_big[0, 64:128], pair_big[1, 64:128]], axis=0).astype(bf16)

    arrived(c_recv.at[pl.ds(0, NZ - 1)], 6)
    top, message = merged([c_recv[i] for i in range(NZ)], lane)
    joined = jnp.maximum(top, self_score)
    fade = jnp.exp(top - joined)
    self_weight = jnp.exp(self_score - joined)
    total = message[:, 65:66] * fade + self_weight
    values = message * fade + self_weight.astype(bf16).astype(f32) * self_value
    head_out = (values / total)[:, :64].astype(bf16)
    d_recv[t] = nn(head_out, w_ao2)
    for u in t_peers:
        send(d_recv.at[t], d_recv.at[t], 7, (z, c, u))
    arrived(d_recv.at[pl.ds(0, NT - 1)], 7)
    total = d_recv[0]
    for i in range(1, NT):
        total = total + d_recv[i]
    resid_mid = resid2 + total
    rm_all[c] = resid_mid
    send(rm_all.at[c], rm_all.at[c], 8, partner)
    square_mid = jnp.broadcast_to(jnp.sum(resid_mid * resid_mid, axis=1, keepdims=True), (8, 128))
    scaled_mid = (resid_mid * gain2).astype(bf16)
    hidden_part = nn(scaled_mid, w_in2)
    for i in range(4):
        for j in range(4):
            e_send[4 * i + j, 0:2] = hidden_part[2 * i : 2 * i + 2, 128 * j : 128 * j + 128]
            e_send[4 * i + j, 2:4] = square_mid[2 * i : 2 * i + 2]
    for peer in z_peers:
        send(e_send.at[peer[0]], e_recv.at[z], 9, peer)
    e_recv[z] = e_send[z]
    arrived(e_recv.at[pl.ds(0, NZ - 1)], 9)
    total = e_recv[0]
    for i in range(1, NZ):
        total = total + e_recv[i]
    inv_mid = lax.rsqrt(total[2:4] / D + EPS)
    hidden = jnp.square(jnp.maximum(inv_mid * total[0:2], 0.0))
    g_recv[z] = hidden
    for peer in z_peers:
        send(g_recv.at[z], g_recv.at[z], 10, peer)
    arrived(g_recv.at[pl.ds(0, NZ - 1)], 10)
    for i in range(4):
        for j in range(4):
            hid_s[2 * i : 2 * i + 2, 128 * j : 128 * j + 128] = g_recv[4 * i + j]
    f_recv[slot] = nt(hid_s[...].astype(bf16), w_out2)
    for peer in plane_peers:
        send(f_recv.at[slot], f_recv.at[slot], 11, peer)
    arrived(rm_all.at[c], 8)
    arrived(f_recv.at[pl.ds(0, 31)], 11)
    for k in (0, 1):
        total = f_recv[k]
        for i in range(1, NT):
            total = total + f_recv[2 * i + k]
        total = rm_all[k] + total
        total = jnp.where(c == 0, total, pltpu.roll(total, 64, 1))
        mixed[8 * k : 8 * k + 8, :] = total[:, :64].astype(bf16)

    sent(pair_a, 0)
    sent(a1.at[pl.ds(0, NZ - 1)], 1)
    sent(pair_small.at[c], 2)
    sent(pair_big.at[c], 3)
    sent(a2.at[pl.ds(0, 31)], 4)
    sent(b_recv.at[pl.ds(0, 31)], 5)
    sent(c_recv.at[pl.ds(0, NZ - 1)], 6)
    sent(d_recv.at[pl.ds(0, NT - 1)], 7)
    sent(rm_all.at[c], 8)
    sent(e_recv.at[pl.ds(0, NZ - 1)], 9)
    sent(g_recv.at[pl.ds(0, NZ - 1)], 10)
    sent(f_recv.at[pl.ds(0, 31)], 11)


def per_device(tokens, lengths, latent, rope, gain_in, w_q, w_kv, w_rope, gain_q, w_qn, w_qr, gain_kv, w_k, w_v, w_ao, gain_mid, w_in, w_out):
    rope = jnp.swapaxes(rope, 1, 2)
    w_rope = w_rope.T
    w_qn = jnp.transpose(w_qn, (1, 2, 0)).reshape(1024, 512)
    w_qr = jnp.transpose(w_qr, (1, 2, 0)).reshape(512, 512)
    w_k = jnp.transpose(w_k, (1, 2, 0)).reshape(1024, 256)
    w_v = jnp.transpose(w_v, (1, 2, 0)).reshape(1024, 256)
    w_out = w_out.T
    steps = np.arange(128) % 16
    freq = jnp.asarray(np.broadcast_to((10000.0 ** (-steps / 16.0)).astype(np.float32), (8, 128)))
    args = (tokens, lengths, latent, rope, gain_in, w_q, w_kv, w_rope, gain_q, w_qn, w_qr, gain_kv, w_k, w_v, w_ao, gain_mid, w_in, w_out, freq)
    places = [pltpu.SMEM((16,), jnp.int32) if a is lengths else pltpu.VMEM(a.shape, a.dtype) for a in args]
    scratch = [
        pltpu.VMEM((32, 4, 128), f32),
        pltpu.VMEM((4, 128), f32),
        pltpu.VMEM((2, 88, 128), f32),
        pltpu.VMEM((2, 128, 512), f32),
        pltpu.VMEM((NZ, 4, 128), f32),
        pltpu.VMEM((32, 4, 128), f32),
        pltpu.VMEM((2, 256, 128), f32),
        pltpu.VMEM((256, 128), f32),
        pltpu.VMEM((2, 256, 128), f32),
        pltpu.VMEM((256, 128), f32),
        pltpu.VMEM((16, 384), f32),
        pltpu.VMEM((32, 8, 128), f32),
        pltpu.VMEM((32, 8, 128), f32),
        pltpu.VMEM((NZ, 8, 128), f32),
        pltpu.VMEM((NT, 8, 128), f32),
        pltpu.VMEM((2, 8, 128), f32),
        pltpu.VMEM((NZ, 4, 128), f32),
        pltpu.VMEM((NZ, 4, 128), f32),
        pltpu.VMEM((NZ, 2, 128), f32),
        pltpu.VMEM((8, 512), f32),
        pltpu.VMEM((32, 8, 128), f32),
        pltpu.SemaphoreType.DMA((len(args),)),
        pltpu.SemaphoreType.DMA((12,)),
        pltpu.SemaphoreType.DMA((12,)),
    ]
    return pl.pallas_call(
        kernel,
        out_shape=(
            jax.ShapeDtypeStruct((16, 64), bf16),
            jax.ShapeDtypeStruct((16, 256), bf16),
            jax.ShapeDtypeStruct((16, 32), bf16),
        ),
        in_specs=[pl.BlockSpec(memory_space=pl.ANY)] * len(args),
        out_specs=tuple([pl.BlockSpec(memory_space=pltpu.VMEM)] * 3),
        scratch_shapes=places + scratch,
        compiler_params=pltpu.CompilerParams(
            collective_id=0, has_side_effects=True, vmem_limit_bytes=48 * 1024 * 1024
        ),
    )(*args)


def solution(mesh):
    finer = Mesh(mesh.devices.reshape(NZ, 2, NT), ("z", "core", "tp"))
    kv, both, tp = ("z", "core"), ("z", "core", "tp"), "tp"
    in_specs = (
        P(None, kv),
        P(),
        P(None, both, None),
        P(None, both, None),
        P(kv),
        P(kv, None),
        P(kv, None),
        P(kv, None),
        P(),
        P(),
        P(),
        P(),
        P(),
        P(),
        P(tp, None, kv),
        P(kv),
        P(kv, tp),
        P(tp, kv),
    )
    return jax.shard_map(
        per_device, mesh=finer, in_specs=in_specs, out_specs=(P(None, kv), P(), P()), check_vma=False
    )
```

time: 242 us -> 85.2 us (0.35); the launches traced: 237 us -> 84.4 us
  blocking collectives: 159 us -> 0 us
  Pallas kernels: 0 us -> 68.3 us
  waiting for transfers between devices: 31.9 us -> 0 us
  starting transfers between devices: 24.2 us -> 0 us
  local copies, waits for them, and re-layouts: 5 us -> 15.5 us
  other arithmetic: 9.57 us -> 0 us
  matrix products: 6.51 us -> 0 us
    psum x6 -> x0, blocking collectives: 94.3 us -> none  [over_axes(): value = lax.psum(value, axis)]
    pallas_call x0 -> x1, Pallas kernels: none -> 68.3 us  [per_device(): pl.pallas_call(kernel, out_shape=(jax.ShapeDtypeStruct((16, 64), bf16), j...]
    all_to_all x1 -> x0, blocking collectives: 64.4 us -> none  [copy_for_each(): lax.all_to_all(jnp.broadcast_to(value[None], (size, *value.shape)), axis,...]
    all_to_all x4 -> x0, waiting for transfers between devices: 31.9 us -> none  [the longest x1 15.2 us: copy_for_each(): lax.all_to_all(jnp.broadcast_to(value[None], (size, *value.shape)), axis,...]
    all_to_all x4 -> x0, starting transfers between devices: 24.2 us -> none  [the longest x1 10.5 us: copy_for_each(): lax.all_to_all(jnp.broadcast_to(value[None], (size, *value.shape)), axis,...]
    unnamed x29 -> x39, local copies, waits for them, and re-layouts: 2.2 us -> 14.8 us
    dot_general x12 -> x0, matrix products: 6.51 us -> none  [the longest x1 1.51 us: per_device(): jnp.einsum('bc,chr->bhr', query_latent, w_up_qr, preferred_element_type=f32)]
    convert_element_type x7 -> x0, other arithmetic: 2.72 us -> none  [the longest x1 0.77 us: per_device(): scaled_in = (resid * gain_in.astype(f32)).astype(bf16)]
  transfers between devices with their start and end apart: 4 -> 0, of which waited for: 4 -> 0; matrix products, arithmetic and copies ran while one was open for 2% -> 0% of each run, Pallas kernels for 0% -> 0%
where the time goes in v1:
time: 85.2 us; the launch traced here: 84.4 us
  Pallas kernels  68.3 us (80%)
  local copies, waits for them, and re-layouts  15.5 us (18%)
    pallas_call x1, Pallas kernels, per_device(): pl.pallas_call(kernel, out_shape=(jax.ShapeDtypeStruct((16, 64), bf16), j...  68.3 us
    unnamed x39, local copies, waits for them, and re-layouts  14.8 us

profile of v1, /device:TPU:1, one launch (start us, length us, event | category | flops | bytes accessed | tf_op | source)
XLA Modules:
  0.0 84.4 jit_solution(14332070891242419829)
XLA Ops:
  0.6 0.0 copy-start.10
  0.6 0.0 copy-start.13
  0.7 0.0 copy-start.14
  0.7 0.7 jit_solution_.3.freq
  1.3 0.0 copy-done.10
  1.3 0.0 copy-done.13
  1.4 0.0 copy-done.14
  1.4 0.0 copy-start
  1.4 1.2 %copy-done = bf16[512,16,64]{0,2,1:T(8,128)(2,1)S(1)} copy-done((bf16[512,16,64]{0,2,1:T(8,128)(2,1)S(1)}, bf16[512,16,64]{0,2,1:T(8,128)(2,1)}, u32[]{:S(2)}) %copy-start) | copy-done | bytes 1048600
  2.6 0.0 copy-start.1
  2.6 1.1 %copy-done.1 = bf16[16,96,256]{2,1,0:T(8,128)(2,1)S(1)} copy-done((bf16[16,96,256]{2,1,0:T(8,128)(2,1)S(1)}, bf16[16,96,256]{2,1,0:T(8,128)(2,1)}, u32[]{:S(2)}) %copy-start.1) | copy-done | bytes 786456
  3.7 0.0 copy-start.2
  3.7 1.0 %copy-done.2 = bf16[512,16,32]{0,2,1:T(8,128)(2,1)S(1)} copy-done((bf16[512,16,32]{0,2,1:T(8,128)(2,1)S(1)}, bf16[512,16,32]{0,2,1:T(8,128)(2,1)}, u32[]{:S(2)}) %copy-start.2) | copy-done | bytes 524312
  4.8 0.0 copy-start.3
  4.8 1.0 %copy-done.3 = bf16[256,16,64]{0,2,1:T(8,128)(2,1)S(1)} copy-done((bf16[256,16,64]{0,2,1:T(8,128)(2,1)S(1)}, bf16[256,16,64]{0,2,1:T(8,128)(2,1)}, u32[]{:S(2)}) %copy-start.3) | copy-done | bytes 524312
  5.8 0.0 copy-start.4
  5.8 1.0 %copy-done.4 = bf16[256,16,64]{0,2,1:T(8,128)(2,1)S(1)} copy-done((bf16[256,16,64]{0,2,1:T(8,128)(2,1)S(1)}, bf16[256,16,64]{0,2,1:T(8,128)(2,1)}, u32[]{:S(2)}) %copy-start.4) | copy-done | bytes 524312
  6.8 0.0 copy-start.5
  6.8 0.9 %copy-done.5 = bf16[16,96,32]{1,2,0:T(8,128)(2,1)S(1)} copy-done((bf16[16,96,32]{1,2,0:T(8,128)(2,1)S(1)}, bf16[16,96,32]{1,2,0:T(8,128)(2,1)}, u32[]{:S(2)}) %copy-start.5) | copy-done | bytes 98328
  7.7 0.8 copy-done.6
  8.6 0.8 copy-done.7
  9.4 0.8 copy-done.8
  10.3 0.8 copy-done.9
  11.0 0.7 copy-done.11
  11.7 0.7 copy-done.12
  12.4 0.7 copy-done.15
  13.1 0.7 copy-done.16
  13.7 0.7 copy-done.17
  14.4 68.3 %shard_map.202 = (bf16[16,64]{1,0:T(8,128)(2,1)S(1)}, bf16[16,256]{1,0:T(8,128)(2,1)S(1)}, bf16[16,32]{1,0:T(8,128)(2,1)S(1)}) custom-call(bf16[16,64]{1,0:T(8,128)(2,1)S(1)} %copy-done.12, s32[16]{0:T(128)S(1)} %copy-done.14, bf16[16,96,256]{2,1,0:T(8,128)(2,1)S(1)} %copy-done.1, bf16[16,32,96]{2,1,0:T(8,128)(2,1)S(1)} %bitcast.19, ...), custom_call_target="tpu_custom_call" | custom-call | tf_op jit(solution)/shard_map/pallas_call | solution.py:432
  82.6 0.6 copy.25
  83.2 0.6 copy.26
  83.8 0.6 copy.27
  (9 shorter events, 0.0 us)
Async XLA Ops:
  0.6 0.7 copy-start.10
  0.6 0.7 copy-start.13
  0.7 0.7 copy-start.14
  1.4 1.2 %copy-start = (bf16[512,16,64]{0,2,1:T(8,128)(2,1)S(1)}, bf16[512,16,64]{0,2,1:T(8,128)(2,1)}, u32[]{:S(2)}) copy-start(bf16[512,16,64]{0,2,1:T(8,128)(2,1)} %param.28) | copy-start | bytes 3145732
  2.6 1.1 %copy-start.1 = (bf16[16,96,256]{2,1,0:T(8,128)(2,1)S(1)}, bf16[16,96,256]{2,1,0:T(8,128)(2,1)}, u32[]{:S(2)}) copy-start(bf16[16,96,256]{2,1,0:T(8,128)(2,1)} %latent.1) | copy-start | bytes 2359300
  3.7 1.0 %copy-start.2 = (bf16[512,16,32]{0,2,1:T(8,128)(2,1)S(1)}, bf16[512,16,32]{0,2,1:T(8,128)(2,1)}, u32[]{:S(2)}) copy-start(bf16[512,16,32]{0,2,1:T(8,128)(2,1)} %param.29) | copy-start | bytes 1572868
  4.8 1.0 %copy-start.3 = (bf16[256,16,64]{0,2,1:T(8,128)(2,1)S(1)}, bf16[256,16,64]{0,2,1:T(8,128)(2,1)}, u32[]{:S(2)}) copy-start(bf16[256,16,64]{0,2,1:T(8,128)(2,1)} %param.31) | copy-start | bytes 1572868
  5.8 1.0 %copy-start.4 = (bf16[256,16,64]{0,2,1:T(8,128)(2,1)S(1)}, bf16[256,16,64]{0,2,1:T(8,128)(2,1)}, u32[]{:S(2)}) copy-start(bf16[256,16,64]{0,2,1:T(8,128)(2,1)} %param.32) | copy-start | bytes 1572868
  6.8 0.9 %copy-start.5 = (bf16[16,96,32]{1,2,0:T(8,128)(2,1)S(1)}, bf16[16,96,32]{1,2,0:T(8,128)(2,1)}, u32[]{:S(2)}) copy-start(bf16[16,96,32]{1,2,0:T(8,128)(2,1)} %param.22) | copy-start | bytes 294916
  7.7 0.8 copy-start.6
  8.6 0.8 copy-start.7
  9.4 0.8 copy-start.8
  10.3 0.8 copy-start.9
  11.0 0.7 copy-start.11
  11.7 0.7 copy-start.12
  12.4 0.7 copy-start.15
  13.1 0.7 copy-start.16
  13.7 0.7 copy-start.17
